TPU v7x, 256 devices: a whole 4x4x8 slice. The times are simulated.
256 devices in a mesh: ep: 64 (over z, y, core), tp: 4 (over x).
Axes of the slice: x: 4, y: 4, z: 8, core: 2. Of those that a mesh axis runs over, the one named last changes fastest.
Arguments:
- cell_query_rows: bfloat16 [16384, 2048], P('ep', 'tp'), may hold values from -6 to 6
- cell_key_rows: bfloat16 [16384, 2048], P('ep', 'tp'), may hold values from -6 to 6
- cell_value_rows: bfloat16 [16384, 2048], P('ep', 'tp'), may hold values from -6 to 6
- output_gate_logits: bfloat16 [16384, 2048], P('ep', 'tp'), may hold values from -8 to 8
- log_input_gate: float32 [8, 16384], P('tp', 'ep'), may hold values from -4 to 110
- forget_gate_logits: float32 [8, 16384], P('tp', 'ep'), may hold values from -1 to 25
- extra_log_forget: float32 [8, 16384], P('tp', 'ep'), may hold values from -0.7 to 0
- cell_output_scale: float32 [2048], P('tp'), may hold values from 0.1 to 1.9
- tokens_into_experts: bfloat16 [32768, 2048], P(('ep', 'tp')), may hold values from -6 to 6
- expert_norm_scale: float32 [2048], replicated, may hold values from 0.1 to 1.9
- token_expert_index: int32 [32768, 2], P(('ep', 'tp')), may hold values from 0 to 63, all different within a row; in each aligned block of 128 rows (0 to 127, 128 to 255, ...) at most 5 rows name the same one
- chosen_expert_weight: float32 [32768, 2], P(('ep', 'tp')), may hold values from 0.3 to 3
- expert_gate_weight: bfloat16 [64, 2048, 3584], P('ep', None, 'tp'), may hold values from -0.125 to 0.125
- expert_up_weight: bfloat16 [64, 2048, 3584], P('ep', None, 'tp'), may hold values from -0.125 to 0.125
- expert_down_weight: bfloat16 [64, 3584, 2048], P('ep', 'tp'), may hold values from -0.09375 to 0.09375
Outputs:
- gated_head_output: bfloat16 [16384, 2048], P('ep', 'tp')
- expert_output: bfloat16 [32768, 2048], P(('ep', 'tp'))
Inputs may be any that keep to these rules, and one draw needn't show every extreme that they name: `token_expert_index`: each row names 2 different experts. Among the rows of one device (aligned blocks of 128 rows) no expert is named by more than 5 rows, and in every draw some expert is named by exactly 5 rows of some device.
All inputs are finite; a program needn't handle non-finite values.
Results may differ from a plain program's by a relative error of at most 0.012.
Values may be sent and summed in bfloat16 or wider, within the bound.
No kernel may reach another device: no remote copies, remote signals or barrier semaphores. Data moves between devices by JAX's collectives and lax.ppermute only.
A program may use at most 128 MiB of HBM per device.

v0:
```python
import jax
import jax.numpy as jnp
from jax import lax
from jax.sharding import Mesh
from jax.sharding import PartitionSpec as P

HEAD_DIM = 256
BLOCK = 64
TOPK = 2
EP = ("ep_0", "ep_1", "ep_2")
EP_TP = ("ep_0", "ep_1", "ep_2", "tp")
EPSILON = 1e-06
PRECISE = lax.Precision.HIGHEST


def nothing_yet(x, identity):
    return jax.tree.map(
        lambda part, zero: jnp.zeros_like(part) + jnp.asarray(zero, part.dtype), x, identity
    )


def collected_together(x, axis):
    leaves = jax.tree.leaves(x)
    turns = sorted(range(len(leaves)), key=lambda k: -leaves[k].size)
    width = (1, *leaves[turns[0]].shape)[-1]
    lines = [
        jnp.pad(leaves[k].reshape(-1), (0, -leaves[k].size % width)).reshape(-1, width)
        for k in turns
    ]
    both, at, found = (lax.all_gather(jnp.concatenate(lines), axis), 0, {})
    for k, line in zip(turns, lines):
        share = both[:, at : at + len(line)].reshape(len(both), -1)
        found[k] = share[:, : leaves[k].size].reshape(-1, *leaves[k].shape)
        at += len(line)
    numbers = iter(range(len(leaves)))
    return jax.tree.map(lambda _: found[next(numbers)], x)


def entering(x, axes, combine, identity):
    before = start = nothing_yet(x, identity)
    so_far = x
    for axis in reversed(axes):
        size, here = (lax.axis_size(axis), lax.axis_index(axis))
        pieces = collected_together(so_far, axis)
        inside, so_far = (start, start)
        for k in range(size):
            passed = k < here
            so_far = combine(so_far, jax.tree.map(lambda part: part[k], pieces))
            inside = jax.tree.map(lambda new, old: jnp.where(passed, new, old), so_far, inside)
        before = combine(inside, before)
    return before


def split_up(x, dim, size):
    before, after = (x.shape[:dim], x.shape[dim + 1 :])
    return jnp.moveaxis(x.reshape(*before, size, -1, *after), dim, 0)


def sum_at_owner(x, axis, dim):
    size = lax.axis_size(axis)
    blocks = lax.all_to_all(split_up(x, dim, size), axis, 0, 0, tiled=True)
    return jnp.sum(blocks.astype(jnp.float32), axis=0)


def combine(earlier, later):
    cell_early, norm_early, stab_early, total_early = earlier
    cell_late, norm_late, stab_late, total_late = later
    stabilizer = jnp.maximum(total_late + stab_early, stab_late)
    keep_factor = jnp.exp(total_late + stab_early - stabilizer)
    take_factor = jnp.exp(stab_late - stabilizer)
    cell_state = (
        keep_factor[..., None, None] * cell_early + take_factor[..., None, None] * cell_late
    )
    norm_state = keep_factor[..., None] * norm_early + take_factor[..., None] * norm_late
    return (cell_state, norm_state, stabilizer, total_early + total_late)


def mix_heads(
    cell_query_rows,
    cell_key_rows,
    cell_value_rows,
    output_gate_logits,
    log_input_gate,
    forget_gate_logits,
    extra_log_forget,
    cell_output_scale,
):
    n_tok, row_width = cell_query_rows.shape
    head_count = row_width // HEAD_DIM
    block_count = n_tok // BLOCK
    key_scale = HEAD_DIM ** (-0.5)
    block_shape = (block_count, BLOCK, head_count, HEAD_DIM)
    query_blocks = cell_query_rows.reshape(block_shape)
    key_blocks = cell_key_rows.reshape(block_shape)
    value_blocks = cell_value_rows.reshape(block_shape)
    gate_input = log_input_gate.reshape(head_count, block_count, BLOCK)
    forget_gate_value = (jax.nn.log_sigmoid(forget_gate_logits) + extra_log_forget).reshape(
        head_count, block_count, BLOCK
    )
    cumulative = jnp.cumsum(forget_gate_value, axis=-1)
    block_last = cumulative[..., -1]
    growth = block_last[..., None] - cumulative + gate_input
    block_top = jnp.max(growth, axis=-1)
    shares = jnp.exp(growth - block_top[..., None])
    key_float = key_blocks.astype(jnp.float32) * key_scale
    value_weighted = value_blocks.astype(jnp.float32) * shares.transpose(1, 2, 0)[..., None]
    cell_terms = jnp.einsum("bshv,bshk->bhvk", value_weighted, key_float, precision=PRECISE)
    norm_terms = jnp.einsum("hbs,bshk->bhk", shares, key_float, precision=PRECISE)
    block_terms = (cell_terms, norm_terms, block_top.T, block_last.T)
    identity_state = (
        jnp.zeros((head_count, HEAD_DIM, HEAD_DIM), jnp.float32),
        jnp.zeros((head_count, HEAD_DIM), jnp.float32),
        jnp.full((head_count,), -1e30, jnp.float32),
        jnp.zeros((head_count,), jnp.float32),
    )

    def fold_step(running, block_term):
        return (combine(running, block_term), running)

    device_total, before = lax.scan(fold_step, identity_state, block_terms)
    prior_state = entering(device_total, EP, combine, identity_state)
    zero_state = (
        jnp.zeros((head_count, HEAD_DIM, HEAD_DIM), jnp.float32),
        jnp.zeros((head_count, HEAD_DIM), jnp.float32),
        jnp.zeros((head_count,), jnp.float32),
        jnp.zeros((head_count,), jnp.float32),
    )
    start_state = combine(zero_state, prior_state)
    cell_state, norm_state, stabilizer, _ = combine(start_state, before)
    inter_log = cumulative + stabilizer.T[:, :, None]
    causal = jnp.tril(jnp.ones((BLOCK, BLOCK), dtype=bool))
    spread = jnp.where(
        causal,
        cumulative[..., :, None] - cumulative[..., None, :] + gate_input[..., None, :],
        -jnp.inf,
    )
    row_top = jnp.maximum(inter_log, jnp.max(spread, axis=-1))
    intra_weight = jnp.exp(spread - row_top[..., None])
    inter_weight = jnp.exp(inter_log - row_top)
    scores = (
        jnp.einsum("bthd,bshd->hbts", query_blocks, key_blocks, preferred_element_type=jnp.float32)
        * key_scale
        * intra_weight
    )
    weights = scores.astype(jnp.bfloat16)
    numerator = jnp.einsum(
        "hbts,bshd->hbtd", weights, value_blocks, preferred_element_type=jnp.float32
    )
    query_float = query_blocks.astype(jnp.float32)
    numerator = numerator + inter_weight[..., None] * jnp.einsum(
        "bhvk,bthk->hbtv", cell_state, query_float, precision=PRECISE
    )
    denominator = jnp.sum(scores, axis=-1) + inter_weight * jnp.einsum(
        "bhk,bthk->hbt", norm_state, query_float, precision=PRECISE
    )
    cell_out = numerator / jnp.maximum(jnp.abs(denominator), 1.0)[..., None]
    cell_out = cell_out.transpose(1, 2, 0, 3).reshape(n_tok, row_width)
    return (
        cell_out * cell_output_scale * jax.nn.sigmoid(output_gate_logits.astype(jnp.float32))
    ).astype(jnp.bfloat16)


def slot_tables(ids, experts, capacity):
    flat_ids = ids.reshape(-1)
    onehot = (flat_ids[:, None] == jnp.arange(experts, dtype=jnp.int32)[None, :]).astype(jnp.int32)
    earlier = jnp.cumsum(onehot, axis=0) - onehot
    rank_in = jnp.sum(earlier * onehot, axis=1)
    slot_index = flat_ids * capacity + rank_in
    token_of = jnp.arange(flat_ids.shape[0], dtype=jnp.int32) // ids.shape[1]
    slot_hit = slot_index[:, None] == jnp.arange(experts * capacity, dtype=jnp.int32)[None, :]
    slot_owner = jnp.sum(jnp.where(slot_hit, token_of[:, None] + 1, 0), axis=0)
    return (slot_owner, slot_index.reshape(ids.shape))


def local(
    cell_query_rows,
    cell_key_rows,
    cell_value_rows,
    output_gate_logits,
    log_input_gate,
    forget_gate_logits,
    extra_log_forget,
    cell_output_scale,
    tokens_into_experts,
    expert_norm_scale,
    token_expert_index,
    chosen_expert_weight,
    expert_gate_weight,
    expert_up_weight,
    expert_down_weight,
):
    gated_head_output = mix_heads(
        cell_query_rows,
        cell_key_rows,
        cell_value_rows,
        output_gate_logits,
        log_input_gate,
        forget_gate_logits,
        extra_log_forget,
        cell_output_scale,
    )
    ep_count = lax.axis_size(EP)
    n_tok = tokens_into_experts.shape[0]
    experts = ep_count * expert_gate_weight.shape[0]
    capacity = n_tok * TOPK * 5 // (4 * experts)
    input_float = tokens_into_experts.astype(jnp.float32)
    normed = (
        input_float
        * lax.rsqrt(jnp.mean(input_float * input_float, axis=-1, keepdims=True) + EPSILON)
        * expert_norm_scale
    ).astype(jnp.bfloat16)
    gate_matrix = expert_gate_weight[0]
    up_matrix = expert_up_weight[0]
    down_matrix = expert_down_weight[0]
    slot_owner, slot_index = slot_tables(token_expert_index, experts, capacity)
    sendbuf = jnp.where(
        (slot_owner > 0)[:, None],
        normed[jnp.maximum(slot_owner - 1, 0)],
        jnp.zeros((), jnp.bfloat16),
    )
    arrived = lax.all_to_all(sendbuf, EP, split_axis=0, concat_axis=0, tiled=True)
    routed_rows = lax.all_gather(arrived, "tp", axis=0, tiled=True)
    gate_out = jnp.dot(routed_rows, gate_matrix, preferred_element_type=jnp.float32)
    up_out = jnp.dot(routed_rows, up_matrix, preferred_element_type=jnp.float32)
    hidden = (jax.nn.silu(gate_out) * up_out).astype(jnp.bfloat16)
    summed = sum_at_owner(
        jnp.dot(hidden, down_matrix, preferred_element_type=jnp.float32).astype(jnp.bfloat16),
        "tp",
        0,
    ).astype(jnp.bfloat16)
    returned = lax.all_to_all(summed, EP, split_axis=0, concat_axis=0, tiled=True)
    picked = returned[slot_index]
    expert_output = jnp.sum(
        chosen_expert_weight[..., None] * picked.astype(jnp.float32), axis=1
    ).astype(jnp.bfloat16)
    return (gated_head_output, expert_output)


def solution(mesh):
    finer = Mesh(mesh.devices.reshape(8, 4, 2, mesh.shape["tp"]), ("ep_0", "ep_1", "ep_2", "tp"))
    placed = (
        P(EP, "tp"),
        P(EP, "tp"),
        P(EP, "tp"),
        P(EP, "tp"),
        P("tp", EP),
        P("tp", EP),
        P("tp", EP),
        P("tp"),
        P(EP_TP, None),
        P(),
        P(EP_TP, None),
        P(EP_TP, None),
        P(EP, None, "tp"),
        P(EP, None, "tp"),
        P(EP, "tp", None),
    )
    return jax.shard_map(
        local, mesh=finer, in_specs=placed, out_specs=(P(EP, "tp"), P(EP_TP, None)), check_vma=False
    )
```

profile of v0, /device:TPU:8, one launch (start us, length us, event | category | flops | bytes accessed | tf_op | source)
XLA Modules:
  0.0 352.7 jit_solution(4525034145210452684)
XLA Ops:
  7.3 0.8 add.1943
  8.0 0.7 fusion.67
  8.9 0.5 reduce_window_sum.28
  9.8 1.0 reshape.3327
  11.0 1.0 reshape.3325
  12.4 2.0 fusion.38
  14.4 17.1 %while.25 = (s32[]{:T(128)}, f32[2,256,256]{2,1,0:T(8,128)S(1)}, f32[2,256]{1,0:T(2,128)S(1)}, f32[2]{0:T(128)S(1)}, f32[2]{0:T(128)S(1)}, /*index=5*/f32[4,2,25...) while((s32[]{:T(128)}, f32[2,256,256]{2,1,0:T(8,128)S(1)}, ...), condition=%wide.region_3.4_spmd.clone, body=%wide.region_2.3_spmd.clone.sunk | while | flops 657939 | bytes 2632044 | solution.py:120
  14.4 0.9 bitcast_dynamic-update-slice_fusion.4
  15.5 0.6 bitcast_dynamic-update-slice_fusion.5
  16.1 1.3 dynamic_update_slice.27
  17.4 1.3 dynamic_update_slice.28
  18.7 0.9 bitcast_dynamic-update-slice_fusion.4
  19.7 0.6 bitcast_dynamic-update-slice_fusion.5
  20.4 1.3 dynamic_update_slice.27
  21.7 1.3 dynamic_update_slice.28
  23.0 0.9 bitcast_dynamic-update-slice_fusion.4
  24.0 0.6 bitcast_dynamic-update-slice_fusion.5
  24.7 1.3 dynamic_update_slice.27
  26.0 1.3 dynamic_update_slice.28
  27.3 0.8 bitcast_dynamic-update-slice_fusion.4
  28.3 0.6 bitcast_dynamic-update-slice_fusion.5
  29.0 1.3 dynamic_update_slice.27
  30.3 1.3 dynamic_update_slice.28
  31.6 0.8 maximum_bitcast_fusion
  33.1 0.6 reduce-window.6
  34.4 15.4 %all-gather.13.cloned.1.call-done = f32[2,516,256]{2,1,0:T(8,128)} async-done(((f32[1,516,256]{2,1,0:T(8,128)}), f32[2,516,256]{2,1,0:T(8,128)}) %all-gather.13.cloned.1.call-update) | async-done | bytes 1056784 | tf_op jit(solution)/shard_map/all_gather | solution.py:30
  49.9 0.8 fusion.135
  51.2 0.8 broadcast_bitcast_fusion.11
  52.0 1.5 fusion.34
  53.6 0.8 maximum_bitcast_fusion.1
  54.5 2.4 gather_fusion
  57.0 0.6 gather.9
  58.0 61.6 %all_to_all.26 = bf16[64,5,2048]{2,1,0:T(8,128)(2,1)S(1)} all-to-all(bf16[64,5,2048]{2,1,0:T(8,128)(2,1)S(1)} %broadcast_select_fusion.3), channel_id=1, replica_groups=mesh['ep_0'=8,'ep_1'=4,'ep_2'=2,'tp'=4] {'ep_0','ep_1','ep_2'}, dimensions={0} | all-to-all | bytes 2621440 | tf_op jit(solution)/shard_map/all_to_all | solution.py:221
  119.6 1.4 all_to_all.18
  121.3 0.8 fusion.133
  122.2 0.6 subtract_exponential_fusion.18
  122.9 0.8 broadcast_bitcast_fusion.7
  123.9 2.0 fusion.27
  125.9 0.9 maximum_bitcast_fusion.2
  126.8 49.9 %all-gather.11.cloned.1.call-done = bf16[1280,2048]{1,0:T(8,128)(2,1)} async-done(((bf16[320,2048]{1,0:T(8,128)(2,1)}), bf16[1280,2048]{1,0:T(8,128)(2,1)}) %all-gather.11.cloned.1.call-update) | async-done | bytes 5242896 | tf_op jit(solution)/shard_map/all_gather | solution.py:222
  176.7 9.9 %fusion.11 = f32[1280,896]{1,0:T(8,128)} fusion(bf16[1280,2048]{1,0:T(8,128)(2,1)} %all-gather.11.cloned.1.call-done, bf16[1,2048,896]{2,1,0:T(8,128)(2,1)} %param.29), kind=kOutput, calls=%fused_computation.26 | convolution fusion | flops 4697620480 | bytes 13500416 | tf_op jit(solution)/shard_map/dot_general | solution.py:223
  186.7 17.7 %convolution_convert_fusion = bf16[1280,2048]{1,0:T(8,128)(2,1)} fusion(bf16[1,896,2048]{2,1,0:T(8,128)(2,1)} %param.31, f32[1280,896]{1,0:T(8,128)} %fusion.11, bf16[1280,2048]{1,0:T(8,128)(2,1)} %all-gather.11.cloned.1.call-done, bf16[1,2048,896]{2,1,0:T(8,128)(2,1)} %param.30), kind=kOutput, calls=%fused_computation.22 | convolution fusion | flops 9404743680 | bytes 22413312 | tf_op jit(solution)/shard_map/dot_general | solution.py:227
  204.4 5.2 %all-to-all-start.1 = ((bf16[4,320,2048]{2,1,0:T(8,128)(2,1)}), bf16[4,320,2048]{2,1,0:T(8,128)(2,1)}, u32[]{:S(2)}, u32[]{:S(2)}) async-start(bf16[4,320,2048]{2,1,0:T(8,128)(2,1)} %bitcast.529), calls=%async_computation.1 | async-start | bytes 10485760 | tf_op jit(solution)/shard_map/all_to_all | solution.py:61
  209.8 0.8 reshape.3324
  210.6 0.7 compare_select_fusion.1
  211.6 0.8 copy.148
  212.6 1.0 fusion.134
  213.9 1.4 fusion.132
  215.3 19.0 %all-gather.17.cloned.1.call-done = f32[8,516,256]{2,1,0:T(8,128)} async-done(((f32[1,516,256]{2,1,0:T(8,128)}), f32[8,516,256]{2,1,0:T(8,128)}) %all-gather.17.cloned.1.call-update) | async-done | bytes 4227088 | tf_op jit(solution)/shard_map/all_gather | solution.py:30
  234.3 0.9 fusion.131
  235.9 1.0 add_bitcast_fusion.2
  236.9 32.8 %all-to-all-done.1 = bf16[4,320,2048]{2,1,0:T(8,128)(2,1)} async-done(((bf16[4,320,2048]{2,1,0:T(8,128)(2,1)}), bf16[4,320,2048]{2,1,0:T(8,128)(2,1)}, u32[]{:S(2)}, u32[]{:S(2)}) %all-to-all-start.1) | async-done | bytes 5242912 | tf_op jit(solution)/shard_map/all_to_all | solution.py:61
  269.7 3.6 %reduce_sum.66 = bf16[320,2048]{1,0:T(8,128)(2,1)S(1)} reduce(bf16[4,320,2048]{2,1,0:T(8,128)(2,1)} %all-to-all-done.1, bf16[]{:T(256)} %constant.113.clone.1), dimensions={0}, to_apply=%region_11.12 | reduce | flops 1966080 | bytes 6553602 | tf_op jit(solution)/shard_map/reduce_sum | solution.py:62
  273.3 1.6 all_to_all.20
  275.0 10.7 %all-to-all-start.2 = ((bf16[64,5,2048]{2,1,0:T(8,128)(2,1)}), bf16[64,5,2048]{2,1,0:T(8,128)(2,1)S(1)}, u32[]{:S(2)}, u32[]{:S(2)}) async-start(bf16[64,5,2048]{2,1,0:T(8,128)(2,1)} %all_to_all.20), calls=%async_computation.2 | async-start | bytes 4194304 | tf_op jit(solution)/shard_map/all_to_all | solution.py:231
  286.5 2.8 fusion.130
  289.5 1.4 multiply_add_fusion.1
  291.1 1.5 fusion.20
  293.5 0.9 multiply_convert_fusion.1
  294.4 42.5 %all-to-all-done.2 = bf16[64,5,2048]{2,1,0:T(8,128)(2,1)S(1)} async-done(((bf16[64,5,2048]{2,1,0:T(8,128)(2,1)}), bf16[64,5,2048]{2,1,0:T(8,128)(2,1)S(1)}, u32[]{:S(2)}, u32[]{:S(2)}) %all-to-all-start.2) | async-done | bytes 1310752 | tf_op jit(solution)/shard_map/all_to_all | solution.py:231
  336.9 0.6 all_to_all.22
  337.5 2.4 gather_fusion.1
  339.9 2.4 reshape.3367
  342.2 3.9 %multiply_reduce_fusion = bf16[128,2048]{1,0:T(8,128)(2,1)} fusion(f32[128,2,2048]{2,1,0:T(2,128)S(1)} %reshape.3367, f32[128,2]{1,0:T(8,128)S(1)} %copy.148), kind=kLoop, calls=%fused_computation.30 | loop fusion | flops 786432 | bytes 2622464 | tf_op jit(solution)/shard_map/reduce_sum | solution.py:233
  (233 shorter events, 8.1 us)
Async XLA Ops:
  7.2 42.7 %all-gather.13.cloned.1.call-start = ((), (), s32[]{:S(2)}) async-start(), calls=%async_computation.4 | async-start | bytes 1597440 | tf_op jit(solution)/shard_map/all_gather | solution.py:30
  10.9 3.6 %copy-start.10 = (bf16[4,64,2,256]{3,2,1,0:T(2,128)(2,1)}, bf16[4,64,2,256]{3,2,1,0:T(2,128)(2,1)S(1)}, u32[]{:S(2)}) copy-start(bf16[4,64,2,256]{3,2,1,0:T(2,128)(2,1)S(1)} %reshape.3327) | copy-start | bytes 786436
  12.0 2.4 copy-start.12
  14.4 18.1 %copy-start.54 = (s32[128,2]{0,1:T(2,128)S(1)}, s32[128,2]{0,1:T(2,128)}, u32[]{:S(2)}) copy-start(s32[128,2]{0,1:T(2,128)} %param.27) | copy-start | bytes 3076
  31.5 1.3 copy-start.2
  31.5 2.7 copy-start.17
  32.4 88.8 %all-gather.15.cloned.1.call-start = ((), (), s32[]{:S(2)}) async-start(), calls=%async_computation.5 | async-start | bytes 2662400 | tf_op jit(solution)/shard_map/all_gather | solution.py:30
  50.7 3.7 %copy-start.32 = (f32[2]{0:T(128)}, f32[2]{0:T(128)S(1)}, u32[]{:S(2)}) copy-start(f32[2]{0:T(128)S(1)} %get-tuple-element.244) | copy-start | bytes 28
  50.7 3.8 %copy-start.41 = (f32[2]{0:T(128)}, f32[2]{0:T(128)S(1)}, u32[]{:S(2)}) copy-start(f32[2]{0:T(128)S(1)} %get-tuple-element.245) | copy-start | bytes 28
  50.7 3.8 %copy-start.36 = (f32[2]{0:T(128)}, f32[2]{0:T(128)S(1)}, u32[]{:S(2)}) copy-start(f32[2]{0:T(128)S(1)} %get-tuple-element.324) | copy-start | bytes 28
  50.7 3.8 %copy-start.38 = (f32[2]{0:T(128)}, f32[2]{0:T(128)S(1)}, u32[]{:S(2)}) copy-start(f32[2]{0:T(128)S(1)} %get-tuple-element.325) | copy-start | bytes 28
  50.8 6.2 %copy-start.34 = (f32[2]{0:T(128)}, f32[2]{0:T(128)S(1)}, u32[]{:S(2)}) copy-start(f32[2]{0:T(128)S(1)} %get-tuple-element.299) | copy-start | bytes 28
  54.4 122.3 %all-gather.11.cloned.1.call-start = ((), (), s32[]{:S(2)}) async-start(), calls=%async_computation.3 | async-start | bytes 6553600 | tf_op jit(solution)/shard_map/all_gather | solution.py:222
  121.0 113.3 %all-gather.17.cloned.1.call-start = ((), (), s32[]{:S(2)}) async-start(), calls=%async_computation.6 | async-start | bytes 4792320 | tf_op jit(solution)/shard_map/all_gather | solution.py:30
  122.1 1.7 copy-start.24
  122.1 1.7 copy-start.43
  122.2 1.7 copy-start.46
  122.2 1.7 copy-start.48
  122.2 1.7 copy-start.50
  122.8 1.0 copy-start.26
  122.8 1.1 copy-start.28
  122.8 1.1 copy-start.30
  122.8 1.0 copy-start.18
  122.8 1.0 copy-start.20
  122.9 1.0 copy-start.22
  204.4 5.4 %copy-start.15 = (bf16[256,512]{1,0:T(8,128)(2,1)S(1)}, bf16[256,512]{1,0:T(8,128)(2,1)}, u32[]{:S(2)}) copy-start(bf16[256,512]{1,0:T(8,128)(2,1)} %param.17) | copy-start | bytes 786436
  204.4 8.2 %copy-start.1 = (f32[2,516,256]{2,1,0:T(8,128)S(1)}, f32[2,516,256]{2,1,0:T(8,128)}, u32[]{:S(2)}) copy-start(f32[2,516,256]{2,1,0:T(8,128)} %all-gather.13.cloned.1.call-done) | copy-start | bytes 3170308
  204.4 65.3 %all-to-all-start.1 = ((bf16[4,320,2048]{2,1,0:T(8,128)(2,1)}), bf16[4,320,2048]{2,1,0:T(8,128)(2,1)}, u32[]{:S(2)}, u32[]{:S(2)}) async-start(bf16[4,320,2048]{2,1,0:T(8,128)(2,1)} %bitcast.529), calls=%async_computation.1 | async-start | bytes 10485760 | tf_op jit(solution)/shard_map/all_to_all | solution.py:61
  209.6 4.1 %copy-start = (f32[4,516,256]{2,1,0:T(8,128)S(1)}, f32[4,516,256]{2,1,0:T(8,128)}, u32[]{:S(2)}) copy-start(f32[4,516,256]{2,1,0:T(8,128)} %all-gather.15.cloned.1.call-done) | copy-start | bytes 6340612
  213.7 21.6 %copy-start.40 = (f32[4,2]{1,0:T(4,128)S(1)}, f32[4,2]{1,0:T(4,128)}, u32[]{:S(2)}) copy-start(f32[4,2]{1,0:T(4,128)} %get-tuple-element.81) | copy-start | bytes 100
  213.7 21.7 %copy-start.56 = (f32[4,2]{1,0:T(4,128)S(1)}, f32[4,2]{1,0:T(4,128)}, u32[]{:S(2)}) copy-start(f32[4,2]{1,0:T(4,128)} %get-tuple-element.76) | copy-start | bytes 100
  213.7 21.9 %copy-start.42 = (f32[2]{0:T(128)S(1)}, f32[2]{0:T(128)}, u32[]{:S(2)}) copy-start(f32[2]{0:T(128)} %copy-done.41) | copy-start | bytes 28
  213.7 21.9 %copy-start.44 = (f32[2]{0:T(128)S(1)}, f32[2]{0:T(128)}, u32[]{:S(2)}) copy-start(f32[2]{0:T(128)} %copy-done.43) | copy-start | bytes 28
  213.7 21.9 %copy-start.47 = (f32[2]{0:T(128)S(1)}, f32[2]{0:T(128)}, u32[]{:S(2)}) copy-start(f32[2]{0:T(128)} %copy-done.46) | copy-start | bytes 28
  213.7 21.9 %copy-start.49 = (f32[2]{0:T(128)S(1)}, f32[2]{0:T(128)}, u32[]{:S(2)}) copy-start(f32[2]{0:T(128)} %copy-done.48) | copy-start | bytes 28
  213.7 21.9 %copy-start.51 = (f32[2]{0:T(128)S(1)}, f32[2]{0:T(128)}, u32[]{:S(2)}) copy-start(f32[2]{0:T(128)} %copy-done.50) | copy-start | bytes 28
  213.7 21.9 %copy-start.53 = (f32[2]{0:T(128)S(1)}, f32[2]{0:T(128)}, u32[]{:S(2)}) copy-start(f32[2]{0:T(128)} %copy-done.52) | copy-start | bytes 28
  213.7 21.9 %copy-start.57 = (f32[2]{0:T(128)S(1)}, f32[2]{0:T(128)}, u32[]{:S(2)}) copy-start(f32[2]{0:T(128)} %get-tuple-element.292) | copy-start | bytes 28
  213.7 21.9 %copy-start.58 = (f32[2]{0:T(128)S(1)}, f32[2]{0:T(128)}, u32[]{:S(2)}) copy-start(f32[2]{0:T(128)} %get-tuple-element.293) | copy-start | bytes 28
  213.7 22.0 %copy-start.19 = (f32[2]{0:T(128)S(1)}, f32[2]{0:T(128)}, u32[]{:S(2)}) copy-start(f32[2]{0:T(128)} %copy-done.18) | copy-start | bytes 28
  213.8 22.0 %copy-start.21 = (f32[2]{0:T(128)S(1)}, f32[2]{0:T(128)}, u32[]{:S(2)}) copy-start(f32[2]{0:T(128)} %copy-done.20) | copy-start | bytes 28
  213.8 22.0 %copy-start.23 = (f32[2]{0:T(128)S(1)}, f32[2]{0:T(128)}, u32[]{:S(2)}) copy-start(f32[2]{0:T(128)} %copy-done.22) | copy-start | bytes 28
  213.8 22.0 %copy-start.25 = (f32[2]{0:T(128)S(1)}, f32[2]{0:T(128)}, u32[]{:S(2)}) copy-start(f32[2]{0:T(128)} %copy-done.24) | copy-start | bytes 28
  213.8 22.0 %copy-start.27 = (f32[2]{0:T(128)S(1)}, f32[2]{0:T(128)}, u32[]{:S(2)}) copy-start(f32[2]{0:T(128)} %copy-done.26) | copy-start | bytes 28
  213.8 22.0 %copy-start.29 = (f32[2]{0:T(128)S(1)}, f32[2]{0:T(128)}, u32[]{:S(2)}) copy-start(f32[2]{0:T(128)} %copy-done.28) | copy-start | bytes 28
  213.8 22.0 %copy-start.31 = (f32[2]{0:T(128)S(1)}, f32[2]{0:T(128)}, u32[]{:S(2)}) copy-start(f32[2]{0:T(128)} %copy-done.30) | copy-start | bytes 28
  213.8 22.0 %copy-start.33 = (f32[2]{0:T(128)S(1)}, f32[2]{0:T(128)}, u32[]{:S(2)}) copy-start(f32[2]{0:T(128)} %copy-done.32) | copy-start | bytes 28
  213.8 22.0 %copy-start.35 = (f32[2]{0:T(128)S(1)}, f32[2]{0:T(128)}, u32[]{:S(2)}) copy-start(f32[2]{0:T(128)} %copy-done.34) | copy-start | bytes 28
  213.8 22.0 %copy-start.37 = (f32[2]{0:T(128)S(1)}, f32[2]{0:T(128)}, u32[]{:S(2)}) copy-start(f32[2]{0:T(128)} %copy-done.36) | copy-start | bytes 28
  213.8 22.0 %copy-start.39 = (f32[2]{0:T(128)S(1)}, f32[2]{0:T(128)}, u32[]{:S(2)}) copy-start(f32[2]{0:T(128)} %copy-done.38) | copy-start | bytes 28
  213.9 23.0 %copy-start.45 = (f32[4,2,256]{2,1,0:T(2,128)S(1)}, f32[4,2,256]{2,1,0:T(2,128)}, u32[]{:S(2)}) copy-start(f32[4,2,256]{2,1,0:T(2,128)} %get-tuple-element.83) | copy-start | bytes 24580
  275.0 10.8 %copy-start.14 = (bf16[4,64,2,256]{3,2,1,0:T(2,128)(2,1)S(1)}, bf16[4,64,2,256]{3,2,1,0:T(2,128)(2,1)}, u32[]{:S(2)}) copy-start(bf16[4,64,2,256]{3,2,1,0:T(2,128)(2,1)} %reshape.3324) | copy-start | bytes 786436
  275.0 11.1 %copy-start.13 = (bf16[4,64,2,256]{3,2,1,0:T(2,128)(2,1)S(1)}, bf16[4,64,2,256]{3,2,1,0:T(2,128)(2,1)}, u32[]{:S(2)}) copy-start(bf16[4,64,2,256]{3,2,1,0:T(2,128)(2,1)} %copy-done.12) | copy-start | bytes 786436
  275.0 61.9 %all-to-all-start.2 = ((bf16[64,5,2048]{2,1,0:T(8,128)(2,1)}), bf16[64,5,2048]{2,1,0:T(8,128)(2,1)S(1)}, u32[]{:S(2)}, u32[]{:S(2)}) async-start(bf16[64,5,2048]{2,1,0:T(8,128)(2,1)} %all_to_all.20), calls=%async_computation.2 | async-start | bytes 4194304 | tf_op jit(solution)/shard_map/all_to_all | solution.py:231
  286.4 2.8 copy-start.3
  286.4 2.8 copy-start.4
  286.4 2.8 copy-start.6
  286.4 2.8 copy-start.7
  286.5 2.9 copy-start.8
  286.5 3.1 copy-start.9
  289.5 1.6 copy-start.5
  291.0 1.6 copy-start.11
  292.6 1.0 copy-start.16
  292.6 0.9 copy-start.55
  (1 other events, 0.5 us)
Sparse Core Ops, SparseCore 0:
  32.5 17.2 all-gather.12
  54.5 50.8 all-gather.14
  121.1 55.5 all-gather.10
  178.4 55.8 all-gather.16
where the time goes:
time: 354 us; the launch traced here: 353 us
  waiting for transfers between devices  160 us (45%)
  blocking collectives  61.6 us (17%)
  local copies, waits for them, and re-layouts  37.3 us (11%)
  matrix products  32.3 us (9%)
  other arithmetic  30.3 us (9%)
  starting transfers between devices  16.3 us (5%)
  between operations  15.1 us (4%)
    all_to_all x1, blocking collectives, local(): lax.all_to_all(sendbuf, EP, split_axis=0, concat_axis=0, tiled=True)  61.6 us
    all_gather x1, waiting for transfers between devices, local(): routed_rows = lax.all_gather(arrived, 'tp', axis=0, tiled=True)  49.9 us
    all_to_all x1, waiting for transfers between devices, local(): lax.all_to_all(summed, EP, split_axis=0, concat_axis=0, tiled=True)  42.5 us
    all_gather x3, waiting for transfers between devices, collected_together(): both, at, found = (lax.all_gather(jnp.concatenate(lines), axis), 0, {})  34.5 us
    all_to_all x1, waiting for transfers between devices, sum_at_owner(): blocks = lax.all_to_all(split_up(x, dim, size), axis, 0, 0, tiled=True)  32.8 us
    dot_general x1, matrix products, local(): jnp.dot(hidden, down_matrix, preferred_element_type=jnp.float32)  17.7 us
    all_to_all x1, starting transfers between devices, local(): lax.all_to_all(summed, EP, split_axis=0, concat_axis=0, tiled=True)  10.7 us
    dynamic_update_slice x8, local copies, waits for them, and re-layouts, mix_heads(): device_total, before = lax.scan(fold_step, identity_state, block_terms)  10.3 us
  transfers between devices with their start and end apart: 6, of which 5 were waited for; matrix products, arithmetic and copies ran while one was open for 15% of the time, Pallas kernels for 0%

commit v1 on v0

--- a/solution.py
+++ b/solution.py
@@ -219,7 +219,11 @@
         jnp.zeros((), jnp.bfloat16),
     )
     arrived = lax.all_to_all(sendbuf, EP, split_axis=0, concat_axis=0, tiled=True)
-    routed_rows = lax.all_gather(arrived, "tp", axis=0, tiled=True)
+    size_2 = lax.axis_size("tp")
+    repeats = [size_2 if d == 0 else 1 for d in range(arrived.ndim)]
+    routed_rows = lax.all_to_all(
+        jnp.tile(arrived, repeats), "tp", split_axis=0, concat_axis=0, tiled=True
+    )
     gate_out = jnp.dot(routed_rows, gate_matrix, preferred_element_type=jnp.float32)
     up_out = jnp.dot(routed_rows, up_matrix, preferred_element_type=jnp.float32)
     hidden = (jax.nn.silu(gate_out) * up_out).astype(jnp.bfloat16)

time: 354 us -> 342 us (0.966)
  blocking collectives: 61.6 us -> 0 us
  waiting for transfers between devices: 160 us -> 192 us
  starting transfers between devices: 16.3 us -> 32.4 us
    all_to_all x0 -> x2, waiting for transfers between devices: none -> 99.6 us  [the longest x1 53.1 us: local(): lax.all_to_all(jnp.tile(arrived, repeats), 'tp', split_axis=0, concat_axi...]
    all_to_all x1 -> x0, blocking collectives: 61.6 us -> none  [local(): lax.all_to_all(sendbuf, EP, split_axis=0, concat_axis=0, tiled=True)]
    all_gather x1 -> x0, waiting for transfers between devices: 49.9 us -> none  [local(): routed_rows = lax.all_gather(arrived, 'tp', axis=0, tiled=True)]
    all_gather x3, waiting for transfers between devices: 34.5 us -> 0.06 us  [collected_together(): both, at, found = (lax.all_gather(jnp.concatenate(lines), axis), 0, {})]
    all_to_all x1, waiting for transfers between devices: 32.8 us -> 52.5 us  [sum_at_owner(): blocks = lax.all_to_all(split_up(x, dim, size), axis, 0, 0, tiled=True)]
    all_to_all x0 -> x2, starting transfers between devices: none -> 17.2 us  [the longest x1 12.1 us: local(): lax.all_to_all(sendbuf, EP, split_axis=0, concat_axis=0, tiled=True)]
    another operation x1 -> x3, local copies, waits for them, and re-layouts: 0.01 us -> 3.63 us  [the longest x2 3.62 us: local(): jnp.tile(arrived, repeats)]
  transfers between devices with their start and end apart: 6 -> 7, of which waited for: 5 -> 4; matrix products, arithmetic and copies ran while one was open for 15% -> 19% of each run, Pallas kernels for 0% -> 0%
where the time goes in v1:
time: 342 us; the launch traced here: 341 us
  waiting for transfers between devices  192 us (56%)
  local copies, waits for them, and re-layouts  37.5 us (11%)
  starting transfers between devices  32.4 us (9%)
  matrix products  32.2 us (9%)
  other arithmetic  31.7 us (9%)
  between operations  15.1 us (4%)
    all_to_all x1, waiting for transfers between devices, local(): lax.all_to_all(jnp.tile(arrived, repeats), 'tp', split_axis=0, concat_axi...  53.1 us
    all_to_all x1, waiting for transfers between devices, sum_at_owner(): blocks = lax.all_to_all(split_up(x, dim, size), axis, 0, 0, tiled=True)  52.5 us
    all_to_all x1, waiting for transfers between devices, local(): lax.all_to_all(sendbuf, EP, split_axis=0, concat_axis=0, tiled=True)  46.6 us
    all_to_all x1, waiting for transfers between devices, local(): lax.all_to_all(summed, EP, split_axis=0, concat_axis=0, tiled=True)  39.8 us
    dot_general x1, matrix products, local(): jnp.dot(hidden, down_matrix, preferred_element_type=jnp.float32)  17.5 us
    all_to_all x1, starting transfers between devices, local(): lax.all_to_all(sendbuf, EP, split_axis=0, concat_axis=0, tiled=True)  12.1 us
    dynamic_update_slice x8, local copies, waits for them, and re-layouts, mix_heads(): device_total, before = lax.scan(fold_step, identity_state, block_terms)  10.3 us
    dot_general x1, matrix products, local(): jnp.dot(routed_rows, gate_matrix, preferred_element_type=jnp.float32)  9.96 us
  transfers between devices with their start and end apart: 7, of which 4 were waited for; matrix products, arithmetic and copies ran while one was open for 19% of the time, Pallas kernels for 0%

profile of v1, /device:TPU:8, one launch (start us, length us, event | category | flops | bytes accessed | tf_op | source)
XLA Modules:
  0.0 341.0 jit_solution(855151945080780182)
XLA Ops:
  7.3 0.8 add.1943
  8.0 0.7 fusion.67
  9.8 1.0 reshape.3335
  11.0 1.0 reshape.3333
  12.4 2.0 fusion.38
  14.4 17.1 %while.25 = (s32[]{:T(128)}, f32[2,256,256]{2,1,0:T(8,128)S(1)}, f32[2,256]{1,0:T(2,128)S(1)}, f32[2]{0:T(128)S(1)}, f32[2]{0:T(128)S(1)}, /*index=5*/f32[4,2,25...) while((s32[]{:T(128)}, f32[2,256,256]{2,1,0:T(8,128)S(1)}, ...), condition=%wide.region_3.4_spmd.clone, body=%wide.region_2.3_spmd.clone.sunk | while | flops 657939 | bytes 2632044 | solution.py:120
  14.4 0.8 bitcast_dynamic-update-slice_fusion.4
  15.5 0.6 bitcast_dynamic-update-slice_fusion.5
  16.2 1.3 dynamic_update_slice.27
  17.4 1.3 dynamic_update_slice.28
  18.7 0.8 bitcast_dynamic-update-slice_fusion.4
  19.8 0.6 bitcast_dynamic-update-slice_fusion.5
  20.4 1.3 dynamic_update_slice.27
  21.7 1.3 dynamic_update_slice.28
  23.0 0.8 bitcast_dynamic-update-slice_fusion.4
  24.0 0.6 bitcast_dynamic-update-slice_fusion.5
  24.7 1.3 dynamic_update_slice.27
  26.0 1.3 dynamic_update_slice.28
  27.3 0.8 bitcast_dynamic-update-slice_fusion.4
  28.3 0.6 bitcast_dynamic-update-slice_fusion.5
  29.0 1.3 dynamic_update_slice.27
  30.2 1.3 dynamic_update_slice.28
  31.6 0.8 maximum_bitcast_fusion
  33.0 0.6 reduce-window.6
  34.4 2.4 gather_fusion
  37.6 1.6 broadcast_select_fusion.3
  39.2 12.1 %all-to-all-start = ((bf16[64,5,2048]{2,1,0:T(8,128)(2,1)}), bf16[64,5,2048]{2,1,0:T(8,128)(2,1)S(1)}, u32[]{:S(2)}, u32[]{:S(2)}) async-start(bf16[64,5,2048]{2,1,0:T(8,128)(2,1)} %broadcast_select_fusion.3), calls=%async_computation | async-start | bytes 4194304 | tf_op jit(solution)/shard_map/all_to_all | solution.py:221
  51.3 0.8 fusion.135
  52.7 0.8 broadcast_bitcast_fusion.11
  53.5 1.5 fusion.34
  55.1 0.8 maximum_bitcast_fusion.1
  56.0 46.6 %all-to-all-done = bf16[64,5,2048]{2,1,0:T(8,128)(2,1)S(1)} async-done(((bf16[64,5,2048]{2,1,0:T(8,128)(2,1)}), bf16[64,5,2048]{2,1,0:T(8,128)(2,1)S(1)}, u32[]{:S(2)}, u32[]{:S(2)}) %all-to-all-start) | async-done | bytes 1310752 | tf_op jit(solution)/shard_map/all_to_all | solution.py:221
  102.5 0.6 tile.4
  103.1 3.1 tile.10
  106.2 5.1 %all-to-all-start.1 = ((bf16[4,320,2048]{2,1,0:T(8,128)(2,1)}), bf16[4,320,2048]{2,1,0:T(8,128)(2,1)}, u32[]{:S(2)}, u32[]{:S(2)}) async-start(bf16[4,320,2048]{2,1,0:T(8,128)(2,1)} %tile.10), calls=%async_computation.1 | async-start | bytes 10485760 | tf_op jit(solution)/shard_map/all_to_all | solution.py:224
  111.5 0.8 fusion.133
  112.4 0.6 subtract_exponential_fusion.18
  113.1 0.8 broadcast_bitcast_fusion.7
  114.1 2.0 fusion.27
  116.1 0.9 maximum_bitcast_fusion.2
  117.0 53.1 %all-to-all-done.1 = bf16[4,320,2048]{2,1,0:T(8,128)(2,1)} async-done(((bf16[4,320,2048]{2,1,0:T(8,128)(2,1)}), bf16[4,320,2048]{2,1,0:T(8,128)(2,1)}, u32[]{:S(2)}, u32[]{:S(2)}) %all-to-all-start.1) | async-done | bytes 5242912 | tf_op jit(solution)/shard_map/all_to_all | solution.py:224
  170.1 10.0 %fusion.11 = f32[1280,896]{1,0:T(8,128)} fusion(bf16[1280,2048]{1,0:T(8,128)(2,1)} %bitcast.87, bf16[1,2048,896]{2,1,0:T(8,128)(2,1)} %param.29), kind=kOutput, calls=%fused_computation.26 | convolution fusion | flops 4697620480 | bytes 13500416 | tf_op jit(solution)/shard_map/dot_general | solution.py:227
  180.1 17.5 %convolution_convert_fusion = bf16[1280,2048]{1,0:T(8,128)(2,1)} fusion(bf16[1,896,2048]{2,1,0:T(8,128)(2,1)} %param.31, f32[1280,896]{1,0:T(8,128)} %fusion.11, bf16[1280,2048]{1,0:T(8,128)(2,1)} %bitcast.87, bf16[1,2048,896]{2,1,0:T(8,128)(2,1)} %param.30), kind=kOutput, calls=%fused_computation.22 | convolution fusion | flops 9404743680 | bytes 22413312 | tf_op jit(solution)/shard_map/dot_general | solution.py:231
  197.6 5.2 %all-to-all-start.2 = ((bf16[4,320,2048]{2,1,0:T(8,128)(2,1)}), bf16[4,320,2048]{2,1,0:T(8,128)(2,1)}, u32[]{:S(2)}, u32[]{:S(2)}) async-start(bf16[4,320,2048]{2,1,0:T(8,128)(2,1)} %bitcast.530), calls=%async_computation.2 | async-start | bytes 10485760 | tf_op jit(solution)/shard_map/all_to_all | solution.py:61
  203.0 0.8 reshape.3332
  203.8 0.7 compare_select_fusion.1
  204.8 0.8 copy.148
  205.8 1.0 fusion.134
  206.9 1.4 fusion.132
  208.3 52.5 %all-to-all-done.2 = bf16[4,320,2048]{2,1,0:T(8,128)(2,1)} async-done(((bf16[4,320,2048]{2,1,0:T(8,128)(2,1)}), bf16[4,320,2048]{2,1,0:T(8,128)(2,1)}, u32[]{:S(2)}, u32[]{:S(2)}) %all-to-all-start.2) | async-done | bytes 5242912 | tf_op jit(solution)/shard_map/all_to_all | solution.py:61
  260.8 3.6 %reduce_sum.66 = bf16[320,2048]{1,0:T(8,128)(2,1)S(1)} reduce(bf16[4,320,2048]{2,1,0:T(8,128)(2,1)} %all-to-all-done.2, bf16[]{:T(256)} %constant.113.clone.1), dimensions={0}, to_apply=%region_11.12 | reduce | flops 1966080 | bytes 6553602 | tf_op jit(solution)/shard_map/reduce_sum | solution.py:62
  264.4 1.6 all_to_all.25
  266.3 9.7 %all-to-all-start.3 = ((bf16[64,5,2048]{2,1,0:T(8,128)(2,1)}), bf16[64,5,2048]{2,1,0:T(8,128)(2,1)S(1)}, u32[]{:S(2)}, u32[]{:S(2)}) async-start(bf16[64,5,2048]{2,1,0:T(8,128)(2,1)} %all_to_all.25), calls=%async_computation.3 | async-start | bytes 4194304 | tf_op jit(solution)/shard_map/all_to_all | solution.py:235
  276.1 0.9 fusion.131
  277.6 1.0 add_bitcast_fusion.2
  279.5 2.8 fusion.130
  282.6 1.4 multiply_add_fusion.1
  284.2 1.5 fusion.20
  286.6 0.9 multiply_convert_fusion.1
  287.4 39.8 %all-to-all-done.3 = bf16[64,5,2048]{2,1,0:T(8,128)(2,1)S(1)} async-done(((bf16[64,5,2048]{2,1,0:T(8,128)(2,1)}), bf16[64,5,2048]{2,1,0:T(8,128)(2,1)S(1)}, u32[]{:S(2)}, u32[]{:S(2)}) %all-to-all-start.3) | async-done | bytes 1310752 | tf_op jit(solution)/shard_map/all_to_all | solution.py:235
  327.3 0.6 all_to_all.27
  327.8 1.4 gather_fusion.1
  329.2 1.3 reshape.3375
  330.5 3.9 %multiply_reduce_fusion = bf16[128,2048]{1,0:T(8,128)(2,1)} fusion(f32[128,2,2048]{2,1,0:T(2,128)S(1)} %reshape.3375, f32[128,2]{1,0:T(8,128)S(1)} %copy.148), kind=kLoop, calls=%fused_computation.30 | loop fusion | flops 786432 | bytes 2622464 | tf_op jit(solution)/shard_map/reduce_sum | solution.py:237
  (234 shorter events, 8.9 us)
Async XLA Ops:
  7.2 44.2 %all-gather.10.cloned.1.call-start = ((), (), s32[]{:S(2)}) async-start(), calls=%async_computation.4 | async-start | bytes 1597440 | tf_op jit(solution)/shard_map/all_gather | solution.py:30
  10.9 3.6 %copy-start.10 = (bf16[4,64,2,256]{3,2,1,0:T(2,128)(2,1)}, bf16[4,64,2,256]{3,2,1,0:T(2,128)(2,1)S(1)}, u32[]{:S(2)}) copy-start(bf16[4,64,2,256]{3,2,1,0:T(2,128)(2,1)S(1)} %reshape.3335) | copy-start | bytes 786436
  12.0 2.4 copy-start.12
  14.4 18.0 %copy-start.54 = (s32[128,2]{0,1:T(2,128)S(1)}, s32[128,2]{0,1:T(2,128)}, u32[]{:S(2)}) copy-start(s32[128,2]{0,1:T(2,128)} %param.27) | copy-start | bytes 3076
  31.5 1.3 copy-start.2
  31.5 2.6 copy-start.17
  39.2 63.3 %all-to-all-start = ((bf16[64,5,2048]{2,1,0:T(8,128)(2,1)}), bf16[64,5,2048]{2,1,0:T(8,128)(2,1)S(1)}, u32[]{:S(2)}, u32[]{:S(2)}) async-start(bf16[64,5,2048]{2,1,0:T(8,128)(2,1)} %broadcast_select_fusion.3), calls=%async_computation | async-start | bytes 4194304 | tf_op jit(solution)/shard_map/all_to_all | solution.py:221
  51.3 60.2 %all-gather.12.cloned.1.call-start = ((), (), s32[]{:S(2)}) async-start(), calls=%async_computation.5 | async-start | bytes 2662400 | tf_op jit(solution)/shard_map/all_gather | solution.py:30
  52.2 1.3 copy-start.41
  52.2 50.9 %copy-start.32 = (f32[2]{0:T(128)}, f32[2]{0:T(128)S(1)}, u32[]{:S(2)}) copy-start(f32[2]{0:T(128)S(1)} %get-tuple-element.244) | copy-start | bytes 28
  52.2 3.7 %copy-start.36 = (f32[2]{0:T(128)}, f32[2]{0:T(128)S(1)}, u32[]{:S(2)}) copy-start(f32[2]{0:T(128)S(1)} %get-tuple-element.324) | copy-start | bytes 28
  52.2 3.7 %copy-start.38 = (f32[2]{0:T(128)}, f32[2]{0:T(128)S(1)}, u32[]{:S(2)}) copy-start(f32[2]{0:T(128)S(1)} %get-tuple-element.325) | copy-start | bytes 28
  52.2 50.9 %copy-start.34 = (f32[2]{0:T(128)}, f32[2]{0:T(128)S(1)}, u32[]{:S(2)}) copy-start(f32[2]{0:T(128)S(1)} %get-tuple-element.299) | copy-start | bytes 28
  106.2 63.9 %all-to-all-start.1 = ((bf16[4,320,2048]{2,1,0:T(8,128)(2,1)}), bf16[4,320,2048]{2,1,0:T(8,128)(2,1)}, u32[]{:S(2)}, u32[]{:S(2)}) async-start(bf16[4,320,2048]{2,1,0:T(8,128)(2,1)} %tile.10), calls=%async_computation.1 | async-start | bytes 10485760 | tf_op jit(solution)/shard_map/all_to_all | solution.py:224
  111.2 164.8 %all-gather.14.cloned.1.call-start = ((), (), s32[]{:S(2)}) async-start(), calls=%async_computation.6 | async-start | bytes 4792320 | tf_op jit(solution)/shard_map/all_gather | solution.py:30
  112.4 1.6 copy-start.24
  112.4 1.6 copy-start.43
  112.4 1.6 copy-start.46
  112.4 1.6 copy-start.48
  112.4 1.6 copy-start.50
  113.0 1.0 copy-start.26
  113.0 1.1 copy-start.28
  113.0 1.1 copy-start.30
  113.1 1.0 copy-start.18
  113.1 1.0 copy-start.20
  113.1 1.0 copy-start.22
  197.6 5.4 %copy-start.15 = (bf16[256,512]{1,0:T(8,128)(2,1)S(1)}, bf16[256,512]{1,0:T(8,128)(2,1)}, u32[]{:S(2)}) copy-start(bf16[256,512]{1,0:T(8,128)(2,1)} %param.17) | copy-start | bytes 786436
  197.6 8.2 %copy-start.1 = (f32[2,516,256]{2,1,0:T(8,128)S(1)}, f32[2,516,256]{2,1,0:T(8,128)}, u32[]{:S(2)}) copy-start(f32[2,516,256]{2,1,0:T(8,128)} %all-gather.10.cloned.1.call-done) | copy-start | bytes 3170308
  197.6 63.2 %all-to-all-start.2 = ((bf16[4,320,2048]{2,1,0:T(8,128)(2,1)}), bf16[4,320,2048]{2,1,0:T(8,128)(2,1)}, u32[]{:S(2)}, u32[]{:S(2)}) async-start(bf16[4,320,2048]{2,1,0:T(8,128)(2,1)} %bitcast.530), calls=%async_computation.2 | async-start | bytes 10485760 | tf_op jit(solution)/shard_map/all_to_all | solution.py:61
  202.8 4.0 %copy-start = (f32[4,516,256]{2,1,0:T(8,128)S(1)}, f32[4,516,256]{2,1,0:T(8,128)}, u32[]{:S(2)}) copy-start(f32[4,516,256]{2,1,0:T(8,128)} %all-gather.12.cloned.1.call-done) | copy-start | bytes 6340612
  266.1 11.0 %copy-start.40 = (f32[4,2]{1,0:T(4,128)S(1)}, f32[4,2]{1,0:T(4,128)}, u32[]{:S(2)}) copy-start(f32[4,2]{1,0:T(4,128)} %get-tuple-element.81) | copy-start | bytes 100
  266.1 11.0 %copy-start.56 = (f32[4,2]{1,0:T(4,128)S(1)}, f32[4,2]{1,0:T(4,128)}, u32[]{:S(2)}) copy-start(f32[4,2]{1,0:T(4,128)} %get-tuple-element.76) | copy-start | bytes 100
  266.1 11.2 %copy-start.42 = (f32[2]{0:T(128)S(1)}, f32[2]{0:T(128)}, u32[]{:S(2)}) copy-start(f32[2]{0:T(128)} %copy-done.41) | copy-start | bytes 28
  266.1 11.2 %copy-start.44 = (f32[2]{0:T(128)S(1)}, f32[2]{0:T(128)}, u32[]{:S(2)}) copy-start(f32[2]{0:T(128)} %copy-done.43) | copy-start | bytes 28
  266.1 11.2 %copy-start.47 = (f32[2]{0:T(128)S(1)}, f32[2]{0:T(128)}, u32[]{:S(2)}) copy-start(f32[2]{0:T(128)} %copy-done.46) | copy-start | bytes 28
  266.1 11.2 %copy-start.49 = (f32[2]{0:T(128)S(1)}, f32[2]{0:T(128)}, u32[]{:S(2)}) copy-start(f32[2]{0:T(128)} %copy-done.48) | copy-start | bytes 28
  266.1 11.2 %copy-start.51 = (f32[2]{0:T(128)S(1)}, f32[2]{0:T(128)}, u32[]{:S(2)}) copy-start(f32[2]{0:T(128)} %copy-done.50) | copy-start | bytes 28
  266.1 11.2 %copy-start.53 = (f32[2]{0:T(128)S(1)}, f32[2]{0:T(128)}, u32[]{:S(2)}) copy-start(f32[2]{0:T(128)} %copy-done.52) | copy-start | bytes 28
  266.1 11.2 %copy-start.57 = (f32[2]{0:T(128)S(1)}, f32[2]{0:T(128)}, u32[]{:S(2)}) copy-start(f32[2]{0:T(128)} %get-tuple-element.292) | copy-start | bytes 28
  266.1 11.2 %copy-start.58 = (f32[2]{0:T(128)S(1)}, f32[2]{0:T(128)}, u32[]{:S(2)}) copy-start(f32[2]{0:T(128)} %get-tuple-element.293) | copy-start | bytes 28
  266.1 11.3 %copy-start.19 = (f32[2]{0:T(128)S(1)}, f32[2]{0:T(128)}, u32[]{:S(2)}) copy-start(f32[2]{0:T(128)} %copy-done.18) | copy-start | bytes 28
  266.2 11.3 %copy-start.21 = (f32[2]{0:T(128)S(1)}, f32[2]{0:T(128)}, u32[]{:S(2)}) copy-start(f32[2]{0:T(128)} %copy-done.20) | copy-start | bytes 28
  266.2 11.3 %copy-start.23 = (f32[2]{0:T(128)S(1)}, f32[2]{0:T(128)}, u32[]{:S(2)}) copy-start(f32[2]{0:T(128)} %copy-done.22) | copy-start | bytes 28
  266.2 11.3 %copy-start.25 = (f32[2]{0:T(128)S(1)}, f32[2]{0:T(128)}, u32[]{:S(2)}) copy-start(f32[2]{0:T(128)} %copy-done.24) | copy-start | bytes 28
  266.2 11.3 %copy-start.27 = (f32[2]{0:T(128)S(1)}, f32[2]{0:T(128)}, u32[]{:S(2)}) copy-start(f32[2]{0:T(128)} %copy-done.26) | copy-start | bytes 28
  266.2 11.3 %copy-start.29 = (f32[2]{0:T(128)S(1)}, f32[2]{0:T(128)}, u32[]{:S(2)}) copy-start(f32[2]{0:T(128)} %copy-done.28) | copy-start | bytes 28
  266.2 11.3 %copy-start.31 = (f32[2]{0:T(128)S(1)}, f32[2]{0:T(128)}, u32[]{:S(2)}) copy-start(f32[2]{0:T(128)} %copy-done.30) | copy-start | bytes 28
  266.2 11.3 %copy-start.33 = (f32[2]{0:T(128)S(1)}, f32[2]{0:T(128)}, u32[]{:S(2)}) copy-start(f32[2]{0:T(128)} %copy-done.32) | copy-start | bytes 28
  266.2 11.3 %copy-start.35 = (f32[2]{0:T(128)S(1)}, f32[2]{0:T(128)}, u32[]{:S(2)}) copy-start(f32[2]{0:T(128)} %copy-done.34) | copy-start | bytes 28
  266.2 11.3 %copy-start.37 = (f32[2]{0:T(128)S(1)}, f32[2]{0:T(128)}, u32[]{:S(2)}) copy-start(f32[2]{0:T(128)} %copy-done.36) | copy-start | bytes 28
  266.2 11.3 %copy-start.39 = (f32[2]{0:T(128)S(1)}, f32[2]{0:T(128)}, u32[]{:S(2)}) copy-start(f32[2]{0:T(128)} %copy-done.38) | copy-start | bytes 28
  266.3 12.4 %copy-start.45 = (f32[4,2,256]{2,1,0:T(2,128)S(1)}, f32[4,2,256]{2,1,0:T(2,128)}, u32[]{:S(2)}) copy-start(f32[4,2,256]{2,1,0:T(2,128)} %get-tuple-element.83) | copy-start | bytes 24580
  266.3 12.5 %copy-start.14 = (bf16[4,64,2,256]{3,2,1,0:T(2,128)(2,1)S(1)}, bf16[4,64,2,256]{3,2,1,0:T(2,128)(2,1)}, u32[]{:S(2)}) copy-start(bf16[4,64,2,256]{3,2,1,0:T(2,128)(2,1)} %reshape.3332) | copy-start | bytes 786436
  266.3 12.8 %copy-start.13 = (bf16[4,64,2,256]{3,2,1,0:T(2,128)(2,1)S(1)}, bf16[4,64,2,256]{3,2,1,0:T(2,128)(2,1)}, u32[]{:S(2)}) copy-start(bf16[4,64,2,256]{3,2,1,0:T(2,128)(2,1)} %copy-done.12) | copy-start | bytes 786436
  266.3 61.0 %all-to-all-start.3 = ((bf16[64,5,2048]{2,1,0:T(8,128)(2,1)}), bf16[64,5,2048]{2,1,0:T(8,128)(2,1)S(1)}, u32[]{:S(2)}, u32[]{:S(2)}) async-start(bf16[64,5,2048]{2,1,0:T(8,128)(2,1)} %all_to_all.25), calls=%async_computation.3 | async-start | bytes 4194304 | tf_op jit(solution)/shard_map/all_to_all | solution.py:235
  279.5 2.8 copy-start.3
  279.5 2.8 copy-start.4
  279.5 2.8 copy-start.6
  279.5 2.8 copy-start.7
  279.5 2.9 copy-start.8
  279.5 3.1 copy-start.9
  282.6 1.6 copy-start.5
  284.0 1.6 copy-start.11
  285.6 1.0 copy-start.16
  (2 other events, 1.5 us)
Sparse Core Ops, SparseCore 0:
  32.5 17.2 all-gather.9
  56.1 46.2 all-gather.11
  117.2 51.7 all-gather.13
